TPU v7x, 32 devices: a whole 2x2x4 slice. The times are simulated.
32 devices in a mesh: ep: 4 (over z), tp: 8 (over y, x, core).
Axes of the slice: x: 2, y: 2, z: 4, core: 2. Of those that a mesh axis runs over, the one named last changes fastest.
Arguments:
- tokens: bfloat16 [32, 4096], P('ep'), may hold values from -6 to 6
- norm_gains: float32 [4, 4096], replicated, may hold values from 0.1 to 1.9
- w_query: bfloat16 [4096, 4096], P(None, 'tp'), may hold values from -0.09375 to 0.09375
- w_query_rope: bfloat16 [4096, 2048], P(None, 'tp'), may hold values from -0.09375 to 0.09375
- w_key_up: bfloat16 [32, 128, 1024], P('tp'), may hold values from -0.5 to 0.5
- w_value_up: bfloat16 [32, 1024, 128], P('tp'), may hold values from -0.1875 to 0.1875
- w_output: bfloat16 [4096, 4096], P('tp'), may hold values from -0.09375 to 0.09375
- w_latent_down: bfloat16 [4096, 1024], P(None, 'tp'), may hold values from -0.09375 to 0.09375
- latent_gain: float32 [1024], replicated, may hold values from 0.1 to 1.9
- w_rope_down: bfloat16 [4096, 64], replicated, may hold values from -0.09375 to 0.09375
- cache_latent: bfloat16 [32, 1024, 1024], P(('ep', 'tp')), may hold values from -300 to 300
- cache_rope: bfloat16 [32, 1024, 64], P(('ep', 'tp')), may hold values from -6 to 6
- lengths: int32 [32], P(('ep', 'tp')), may hold values from 1 to 1024, as said below
- routes: int32 [32, 2], P('ep'), may hold values from 0 to 3, all different within a row; in each aligned block of 8 rows (0 to 7, 8 to 15, ...) at most 7 rows name the same one
- route_weights: float32 [32, 2], P('ep'), may hold values from 0.2 to 1
- w_gate: bfloat16 [4, 4096, 2048], P('ep', None, 'tp'), may hold values from -0.09375 to 0.09375
- w_up: bfloat16 [4, 4096, 2048], P('ep', None, 'tp'), may hold values from -0.09375 to 0.09375
- w_down: bfloat16 [4, 2048, 4096], P('ep', 'tp'), may hold values from -0.125 to 0.125
Outputs:
- hidden_out: bfloat16 [32, 4096], P(('ep', 'tp'))
- new_latent: bfloat16 [32, 1024], P(('ep', 'tp'))
- new_rope: bfloat16 [32, 64], P(('ep', 'tp'))
Inputs may be any that keep to these rules, and one draw needn't show every extreme that they name: `routes`: within each aligned block of 8 rows no expert is named by more than 7 rows, a bound that some block reaches; the 2 experts of a row differ. The new token stands at position lengths; some sequence has exactly 1024.
All inputs are finite; a program needn't handle non-finite values.
Results may differ from a plain program's by a relative error of at most 0.02.
Values may be sent and summed in bfloat16 or wider, within the bound.
A program may use at most 64 MiB of HBM per device.

v0:
```python
import jax
import jax.numpy as jnp
from jax import lax
from jax.sharding import PartitionSpec as P

EXP_LOCAL = 1
EPSILON = 1e-06
ROTARY_BASE = 500000.0


def rms_scale(source, gain_row):
    values_f = source.astype(jnp.float32)
    return (
        values_f
        * lax.rsqrt(jnp.mean(values_f * values_f, axis=-1, keepdims=True) + EPSILON)
        * gain_row
    )


def rotate(source, position):
    half_width = source.shape[-1] // 2
    frequency = ROTARY_BASE ** (-jnp.arange(half_width, dtype=jnp.float32) / half_width)
    angles = position[..., None] * frequency
    first_half = source[..., :half_width]
    second_half = source[..., half_width:]
    return jnp.concatenate(
        [
            first_half * jnp.cos(angles) - second_half * jnp.sin(angles),
            second_half * jnp.cos(angles) + first_half * jnp.sin(angles),
        ],
        axis=-1,
    )


def attend(q_latent, q_pe, cache_lat, cache_rp, lat_new, rope_new, lengths, score_scale):
    scores = (
        jnp.einsum("shc,spc->shp", q_latent, cache_lat, preferred_element_type=jnp.float32)
        + jnp.einsum("shr,spr->shp", q_pe, cache_rp, preferred_element_type=jnp.float32)
    ) * score_scale
    own_score = (
        jnp.einsum("shc,sc->sh", q_latent, lat_new, preferred_element_type=jnp.float32)
        + jnp.einsum("shr,sr->sh", q_pe, rope_new, preferred_element_type=jnp.float32)
    ) * score_scale
    visible = (
        jnp.arange(cache_lat.shape[1], dtype=jnp.int32)[None, None, :] < lengths[:, None, None]
    )
    row_max = jnp.maximum(jnp.max(jnp.where(visible, scores, -jnp.inf), axis=-1), own_score)
    weights = jnp.where(visible, jnp.exp(scores - row_max[..., None]), 0.0)
    own_weight = jnp.exp(own_score - row_max)
    denominator = jnp.sum(weights, axis=-1) + own_weight
    probabilities = (weights / denominator[..., None]).astype(jnp.bfloat16)
    own_prob = (own_weight / denominator).astype(jnp.bfloat16)
    attended = jnp.einsum(
        "shp,spc->shc", probabilities, cache_lat, preferred_element_type=jnp.float32
    )
    attended = (
        attended + own_prob.astype(jnp.float32)[..., None] * lat_new.astype(jnp.float32)[:, None, :]
    )
    return attended.astype(jnp.bfloat16)


def on_device(
    tokens,
    norm_gains,
    w_query,
    w_query_rope,
    w_key_up,
    w_value_up,
    w_output,
    w_latent_down,
    latent_gain,
    w_rope_down,
    cache_latent,
    cache_rope,
    lengths,
    routes,
    route_weights,
    w_gate,
    w_up,
    w_down,
):
    group_rows = tokens.shape[0]
    seq_count = cache_latent.shape[0]
    heads_here = w_key_up.shape[0]
    nope_width = w_key_up.shape[1]
    rope_width = w_rope_down.shape[1]
    tp_size = lax.axis_size("tp")
    tp_rank = lax.axis_index("tp")
    normed = rms_scale(tokens, norm_gains[0]).astype(jnp.bfloat16)
    q_nope = jnp.dot(normed, w_query, preferred_element_type=jnp.float32).astype(jnp.bfloat16)
    q_nope = q_nope.reshape(group_rows, heads_here, nope_width)
    q_latent = jnp.einsum("thn,hnc->thc", q_nope, w_key_up, preferred_element_type=jnp.float32)
    q_latent = q_latent.astype(jnp.bfloat16).reshape(group_rows, -1)
    q_rot = jnp.dot(normed, w_query_rope, preferred_element_type=jnp.float32).astype(jnp.bfloat16)
    latent_cols = jnp.dot(normed, w_latent_down, preferred_element_type=jnp.float32).astype(
        jnp.bfloat16
    )
    q_mine, rot_mine, latent_raw = (
        lax.all_to_all(q_latent, "tp", split_axis=0, concat_axis=1, tiled=True),
        lax.all_to_all(q_rot, "tp", split_axis=0, concat_axis=1, tiled=True),
        lax.all_to_all(latent_cols, "tp", split_axis=0, concat_axis=1, tiled=True),
    )
    heads_all = rot_mine.shape[1] // rope_width
    own_normed = lax.dynamic_slice_in_dim(normed, tp_rank * seq_count, seq_count, 0)
    rope_raw = jnp.dot(own_normed, w_rope_down, preferred_element_type=jnp.float32).astype(
        jnp.bfloat16
    )
    new_latent = rms_scale(latent_raw, latent_gain).astype(jnp.bfloat16)
    position = lengths.astype(jnp.float32)
    new_rope = rotate(rope_raw.astype(jnp.float32), position).astype(jnp.bfloat16)
    q_pe = rotate(
        rot_mine.reshape(seq_count, heads_all, rope_width).astype(jnp.float32), position[:, None]
    )
    q_pe = q_pe.astype(jnp.bfloat16)
    score_scale = (nope_width + rope_width) ** (-0.5)
    attended = attend(
        q_mine.reshape(seq_count, heads_all, -1),
        q_pe,
        cache_latent,
        cache_rope,
        new_latent,
        new_rope,
        lengths,
        score_scale,
    )
    head_latent = lax.all_to_all(
        attended.reshape(seq_count, -1), "tp", split_axis=1, concat_axis=0, tiled=True
    )
    values = (
        jnp.einsum(
            "thc,hcv->thv",
            head_latent.reshape(group_rows, heads_here, -1),
            w_value_up,
            preferred_element_type=jnp.float32,
        )
        .astype(jnp.bfloat16)
        .reshape(group_rows, -1)
    )
    head_term = jnp.dot(values, w_output, preferred_element_type=jnp.float32)
    mixed = lax.psum(head_term.astype(jnp.bfloat16), "tp").astype(jnp.float32)
    resid = (tokens.astype(jnp.float32) + rms_scale(mixed, norm_gains[1])).astype(jnp.bfloat16)
    expert_in = rms_scale(resid, norm_gains[2]).astype(jnp.bfloat16)
    own_resid = lax.dynamic_slice_in_dim(resid, tp_rank * seq_count, seq_count, 0)
    ep_size = lax.axis_size("ep")
    experts = ep_size * EXP_LOCAL
    local_expert = tp_rank // (tp_size // EXP_LOCAL)
    route_count = routes.shape[1]
    capacity = (
        (group_rows * route_count + experts - 1) // experts
        + 2
        + group_rows * route_count // (4 * experts)
    )
    slot_count = ep_size * capacity
    flat_routes = routes.reshape(-1)
    expert_hits = (flat_routes[:, None] == jnp.arange(experts, dtype=jnp.int32)[None, :]).astype(
        jnp.int32
    )
    slot_rank = jnp.sum((jnp.cumsum(expert_hits, axis=0) - 1) * expert_hits, axis=1)
    served_here = flat_routes % EXP_LOCAL == local_expert
    slot_index = jnp.where(served_here, flat_routes // EXP_LOCAL * capacity + slot_rank, -1)
    slot_picks = (slot_index[:, None] == jnp.arange(slot_count, dtype=jnp.int32)[None, :]).astype(
        jnp.bfloat16
    )
    slot_picks = slot_picks.reshape(group_rows, route_count, slot_count)
    slot_rows = jnp.sum(slot_picks, axis=1)
    outgoing = jnp.dot(slot_rows.T, expert_in, preferred_element_type=jnp.float32).astype(
        jnp.bfloat16
    )
    arrived = lax.all_to_all(outgoing, "ep", split_axis=0, concat_axis=0, tiled=True)
    gate_sum = jnp.dot(arrived, w_gate[0], preferred_element_type=jnp.float32)
    up_sum = jnp.dot(arrived, w_up[0], preferred_element_type=jnp.float32)
    hidden_units = (jax.nn.silu(gate_sum) * up_sum).astype(jnp.bfloat16)
    expert_out = jnp.dot(hidden_units, w_down[0], preferred_element_type=jnp.float32).astype(
        jnp.bfloat16
    )
    returned = lax.all_to_all(expert_out, "ep", split_axis=0, concat_axis=0, tiled=True)
    routed_part = jnp.zeros((group_rows, returned.shape[1]), jnp.float32)
    for route_slot in range(route_count):
        chosen = jnp.dot(slot_picks[:, route_slot, :], returned, preferred_element_type=jnp.float32)
        routed_part = routed_part + route_weights[:, route_slot : route_slot + 1] * chosen
    routed = lax.psum_scatter(
        routed_part.astype(jnp.bfloat16), "tp", scatter_dimension=0, tiled=True
    ).astype(jnp.float32)
    hidden_out = (own_resid.astype(jnp.float32) + rms_scale(routed, norm_gains[3])).astype(
        jnp.bfloat16
    )
    return (hidden_out, new_latent, new_rope)


def solution(mesh):
    in_specs = (
        P("ep", None),
        P(),
        P(None, "tp"),
        P(None, "tp"),
        P("tp", None, None),
        P("tp", None, None),
        P("tp", None),
        P(None, "tp"),
        P(),
        P(),
        P(("ep", "tp"), None, None),
        P(("ep", "tp"), None, None),
        P(("ep", "tp")),
        P("ep", None),
        P("ep", None),
        P("ep", None, "tp"),
        P("ep", None, "tp"),
        P("ep", "tp", None),
    )
    out_specs = (P(("ep", "tp"), None), P(("ep", "tp"), None), P(("ep", "tp"), None))
    return jax.shard_map(
        on_device, mesh=mesh, in_specs=in_specs, out_specs=out_specs, check_vma=False
    )
```

profile of v0, /device:TPU:0, one launch (start us, length us, event | category | flops | bytes accessed | tf_op | source)
XLA Modules:
  0.0 212.2 jit_solution(539098069489857588)
XLA Ops:
  7.2 1.1 fusion.78
  8.3 1.0 fusion.40
  9.3 0.9 fusion.42
  10.2 1.5 fusion.29
  11.7 0.6 copy.35
  12.3 5.2 %all-to-all-start.2 = ((bf16[8,1,128]{2,1,0:T(2,128)(2,1)}), bf16[8,1,128]{2,1,0:T(2,128)(2,1)S(1)}, u32[]{:S(2)}, u32[]{:S(2)}) async-start(bf16[8,1,128]{2,1,0:T(2,128)(2,1)} %copy.35), calls=%async_computation.2 | async-start | bytes 8192 | tf_op jit(solution)/shard_map/all_to_all | solution.py:101
  17.5 2.0 fusion.28
  20.2 1.3 fusion.34
  22.1 3.1 %convolution_convert_fusion.3 = bf16[4,8,1024]{2,1,0:T(8,128)(2,1)S(1)} fusion(bf16[4,128,1024]{2,1,0:T(8,128)(2,1)S(1)} %copy-done.2, bf16[8,4096]{1,0:T(8,128)(2,1)S(1)} %fusion.42, bf16[4096,512]{1,0:T(8,128)(2,1)} %param.20), kind=kOutput, calls=%fused_computation.20 | convolution fusion | flops 41979904 | bytes 5373952 | tf_op jit(solution)/shard_map/thn,hnc->thc/dot_general | solution.py:92
  25.1 0.5 broadcast.263
  25.7 0.6 reduce.13
  26.3 0.6 reshape.355
  26.9 0.7 reduce.12
  27.6 0.7 reshape.353
  28.3 4.2 %all-to-all-start.1 = ((bf16[8,2,128]{2,1,0:T(2,128)(2,1)}), bf16[8,2,128]{2,1,0:T(2,128)(2,1)S(1)}, u32[]{:S(2)}, u32[]{:S(2)}) async-start(bf16[8,2,128]{2,1,0:T(2,128)(2,1)} %reshape.355), calls=%async_computation.1 | async-start | bytes 8192 | tf_op jit(solution)/shard_map/all_to_all | solution.py:100
  32.5 0.6 multiply_reduce_fusion.1
  33.9 3.3 %all-to-all-done.1 = bf16[8,2,128]{2,1,0:T(2,128)(2,1)S(1)} async-done(((bf16[8,2,128]{2,1,0:T(2,128)(2,1)}), bf16[8,2,128]{2,1,0:T(2,128)(2,1)S(1)}, u32[]{:S(2)}, u32[]{:S(2)}) %all-to-all-start.1) | async-done | bytes 4128 | tf_op jit(solution)/shard_map/all_to_all | solution.py:100
  37.1 3.3 %all-to-all-start = ((bf16[8,2,2048]{2,1,0:T(2,128)(2,1)}), bf16[8,2,2048]{2,1,0:T(2,128)(2,1)S(1)}, u32[]{:S(2)}, u32[]{:S(2)}) async-start(bf16[8,2,2048]{2,1,0:T(2,128)(2,1)} %reshape.353), calls=%async_computation | async-start | bytes 131072 | tf_op jit(solution)/shard_map/all_to_all | solution.py:99
  40.7 4.8 %all-to-all-done = bf16[8,2,2048]{2,1,0:T(2,128)(2,1)S(1)} async-done(((bf16[8,2,2048]{2,1,0:T(2,128)(2,1)}), bf16[8,2,2048]{2,1,0:T(2,128)(2,1)S(1)}, u32[]{:S(2)}, u32[]{:S(2)}) %all-to-all-start) | async-done | bytes 65568 | tf_op jit(solution)/shard_map/all_to_all | solution.py:99
  45.5 0.4 reduce.7
  46.0 2.5 %fusion.9 = f32[32,1024]{1,0:T(8,128)S(1)} fusion(bf16[32,1024]{1,0:T(8,128)(2,1)S(1)} %reshape.334, bf16[1,1024,1024]{2,1,0:T(8,128)(2,1)} %param.28), kind=kOutput, calls=%fused_computation.14 | convolution fusion | flops 67108864 | bytes 2293760 | tf_op jit(solution)/shard_map/shc,spc->shp/dot_general | solution.py:37
  48.6 0.3 select_reduce_fusion
  48.9 0.2 fusion.79
  49.1 0.2 fusion.45
  49.3 0.5 fusion.15
  49.9 1.0 reduce.14
  50.9 0.7 reshape.357
  51.6 3.3 %all-to-all-start.3 = ((bf16[8,2,2048]{2,1,0:T(2,128)(2,1)}), bf16[8,2,2048]{2,1,0:T(2,128)(2,1)S(1)}, u32[]{:S(2)}, u32[]{:S(2)}) async-start(bf16[8,2,2048]{2,1,0:T(2,128)(2,1)} %reshape.357), calls=%async_computation.3 | async-start | bytes 131072 | tf_op jit(solution)/shard_map/all_to_all | solution.py:126
  55.1 4.8 %all-to-all-done.3 = bf16[8,2,2048]{2,1,0:T(2,128)(2,1)S(1)} async-done(((bf16[8,2,2048]{2,1,0:T(2,128)(2,1)}), bf16[8,2,2048]{2,1,0:T(2,128)(2,1)S(1)}, u32[]{:S(2)}, u32[]{:S(2)}) %all-to-all-start.3) | async-done | bytes 65568 | tf_op jit(solution)/shard_map/all_to_all | solution.py:126
  59.9 0.4 bitcast_reduce_fusion
  60.3 3.7 %convolution_convert_fusion.2 = bf16[8,4096]{1,0:T(8,128)(2,1)} fusion(bf16[512,4096]{1,0:T(8,128)(2,1)} %param.24, bf16[8,4,1024]{2,0,1:T(8,128)(2,1)S(1)} %bitcast.123, bf16[4,1024,128]{2,1,0:T(8,128)(2,1)S(1)} %copy-done.3), kind=kOutput, calls=%fused_computation.6 | convolution fusion | flops 41979904 | bytes 5373952 | tf_op jit(solution)/shard_map/dot_general | solution.py:139
  64.1 52.6 %all-reduce.4.cloned.1.call-done = bf16[8,4096]{1,0:T(8,128)(2,1)} async-done(((bf16[8,4096]{1,0:T(8,128)(2,1)}), bf16[8,4096]{1,0:T(8,128)(2,1)}) %all-reduce.4.cloned.1.call-update) | async-done | bytes 65552 | tf_op jit(solution)/shard_map/psum | solution.py:140
  116.7 1.0 fusion.35
  117.7 1.1 fusion.37
  118.8 0.3 convolution_convert_fusion.1
  119.2 12.5 %all_to_all.77 = bf16[4,7,4096]{2,1,0:T(8,128)(2,1)S(1)} all-to-all(bf16[4,7,4096]{2,1,0:T(8,128)(2,1)S(1)} %all_to_all.64), channel_id=1, replica_groups=mesh['ep'=4,'tp'=8] {'ep'}, dimensions={0} | all-to-all | bytes 458752 | tf_op jit(solution)/shard_map/all_to_all | solution.py:169
  131.8 2.1 fusion.5
  133.9 2.9 %convolution_convert_fusion = bf16[28,4096]{1,0:T(8,128)(2,1)S(1)} fusion(bf16[1,256,4096]{2,1,0:T(8,128)(2,1)S(1)} %copy-done, bf16[28,4096]{1,0:T(8,128)(2,1)S(1)} %all_to_all.66, bf16[1,4096,256]{2,1,0:T(8,128)(2,1)} %param.34, f32[28,256]{1,0:T(8,128)S(1)} %fusion.5), kind=kOutput, calls=%fused_computation | convolution fusion | flops 117598208 | bytes 4681728 | tf_op jit(solution)/shard_map/dot_general | solution.py:173
  136.7 0.8 all_to_all.67
  137.5 3.4 %all-to-all-start.5 = ((bf16[4,7,4096]{2,1,0:T(8,128)(2,1)}), bf16[4,7,4096]{2,1,0:T(8,128)(2,1)S(1)}, u32[]{:S(2)}, u32[]{:S(2)}) async-start(bf16[4,7,4096]{2,1,0:T(8,128)(2,1)} %all_to_all.67), calls=%async_computation.5 | async-start | bytes 524288 | tf_op jit(solution)/shard_map/all_to_all | solution.py:176
  141.1 7.7 %all-to-all-done.5 = bf16[4,7,4096]{2,1,0:T(8,128)(2,1)S(1)} async-done(((bf16[4,7,4096]{2,1,0:T(8,128)(2,1)}), bf16[4,7,4096]{2,1,0:T(8,128)(2,1)S(1)}, u32[]{:S(2)}, u32[]{:S(2)}) %all-to-all-start.5) | async-done | bytes 229408 | tf_op jit(solution)/shard_map/all_to_all | solution.py:176
  149.1 0.8 fusion.1
  149.9 0.6 pad_maximum_fusion.3
  150.4 0.6 dynamic-slice
  151.0 0.6 convert_element_type.184
  151.6 48.9 %all-reduce.6.cloned.1.call-done = bf16[8,4096]{1,0:T(8,128)(2,1)} async-done(((bf16[8,4096]{1,0:T(8,128)(2,1)}), bf16[8,4096]{1,0:T(8,128)(2,1)}) %all-reduce.6.cloned.1.call-update) | async-done | bytes 65552
  200.5 2.0 multiply_reduce_fusion
  203.2 2.1 add_convert_fusion
  (59 shorter events, 2.1 us)
Async XLA Ops:
  7.2 126.7 %copy-start = (bf16[1,256,4096]{2,1,0:T(8,128)(2,1)S(1)}, bf16[1,256,4096]{2,1,0:T(8,128)(2,1)}, u32[]{:S(2)}) copy-start(bf16[1,256,4096]{2,1,0:T(8,128)(2,1)} %param.35) | copy-start | bytes 6291460
  7.2 14.4 %copy-start.7 = (s32[8,2]{0,1:T(2,128)S(1)}, s32[8,2]{0,1:T(2,128)}, u32[]{:S(2)}) copy-start(s32[8,2]{0,1:T(2,128)} %param.31) | copy-start | bytes 196
  7.2 14.8 %copy-start.2 = (bf16[4,128,1024]{2,1,0:T(8,128)(2,1)S(1)}, bf16[4,128,1024]{2,1,0:T(8,128)(2,1)}, u32[]{:S(2)}) copy-start(bf16[4,128,1024]{2,1,0:T(8,128)(2,1)} %param.22) | copy-start | bytes 3145732
  12.3 16.0 %all-to-all-start.2 = ((bf16[8,1,128]{2,1,0:T(2,128)(2,1)}), bf16[8,1,128]{2,1,0:T(2,128)(2,1)S(1)}, u32[]{:S(2)}, u32[]{:S(2)}) async-start(bf16[8,1,128]{2,1,0:T(2,128)(2,1)} %copy.35), calls=%async_computation.2 | async-start | bytes 8192 | tf_op jit(solution)/shard_map/all_to_all | solution.py:101
  22.0 11.8 %copy-start.6 = (f32[1024]{0:T(1024)S(1)}, f32[1024]{0:T(1024)}, u32[]{:S(2)}) copy-start(f32[1024]{0:T(1024)} %param.26) | copy-start | bytes 12292
  25.1 23.4 %copy-start.5 = (bf16[1,1024,64]{1,2,0:T(8,128)(2,1)S(1)}, bf16[1,1024,64]{1,2,0:T(8,128)(2,1)}, u32[]{:S(2)}) copy-start(bf16[1,1024,64]{1,2,0:T(8,128)(2,1)} %param.29) | copy-start | bytes 393220
  28.3 8.8 %all-to-all-start.1 = ((bf16[8,2,128]{2,1,0:T(2,128)(2,1)}), bf16[8,2,128]{2,1,0:T(2,128)(2,1)S(1)}, u32[]{:S(2)}, u32[]{:S(2)}) async-start(bf16[8,2,128]{2,1,0:T(2,128)(2,1)} %reshape.355), calls=%async_computation.1 | async-start | bytes 8192 | tf_op jit(solution)/shard_map/all_to_all | solution.py:100
  37.1 8.3 %all-to-all-start = ((bf16[8,2,2048]{2,1,0:T(2,128)(2,1)}), bf16[8,2,2048]{2,1,0:T(2,128)(2,1)S(1)}, u32[]{:S(2)}, u32[]{:S(2)}) async-start(bf16[8,2,2048]{2,1,0:T(2,128)(2,1)} %reshape.353), calls=%async_computation | async-start | bytes 131072 | tf_op jit(solution)/shard_map/all_to_all | solution.py:99
  45.9 3.4 %copy-start.1 = (bf16[1,1024,1024]{2,1,0:T(8,128)(2,1)S(1)}, bf16[1,1024,1024]{2,1,0:T(8,128)(2,1)}, u32[]{:S(2)}) copy-start(bf16[1,1024,1024]{2,1,0:T(8,128)(2,1)} %param.28) | copy-start | bytes 6291460
  48.4 11.9 %copy-start.3 = (bf16[4,1024,128]{2,1,0:T(8,128)(2,1)S(1)}, bf16[4,1024,128]{2,1,0:T(8,128)(2,1)}, u32[]{:S(2)}) copy-start(bf16[4,1024,128]{2,1,0:T(8,128)(2,1)} %param.23) | copy-start | bytes 3145732
  51.6 8.3 %all-to-all-start.3 = ((bf16[8,2,2048]{2,1,0:T(2,128)(2,1)}), bf16[8,2,2048]{2,1,0:T(2,128)(2,1)S(1)}, u32[]{:S(2)}, u32[]{:S(2)}) async-start(bf16[8,2,2048]{2,1,0:T(2,128)(2,1)} %reshape.357), calls=%async_computation.3 | async-start | bytes 131072 | tf_op jit(solution)/shard_map/all_to_all | solution.py:126
  54.9 61.8 %all-reduce.4.cloned.1.call-start = ((), (), s32[]{:S(2)}) async-start(), calls=%async_computation.6 | async-start | bytes 131072 | tf_op jit(solution)/shard_map/psum | solution.py:140
  60.3 57.4 %copy-start.4 = (bf16[8,4096]{1,0:T(8,128)(2,1)S(1)}, bf16[8,4096]{1,0:T(8,128)(2,1)}, u32[]{:S(2)}) copy-start(bf16[8,4096]{1,0:T(8,128)(2,1)} %param.18) | copy-start | bytes 196612
  133.8 7.1 %copy-start.8 = (f32[8,2]{0,1:T(2,128)S(1)}, f32[8,2]{0,1:T(2,128)}, u32[]{:S(2)}) copy-start(f32[8,2]{0,1:T(2,128)} %param.32) | copy-start | bytes 196
  136.7 13.7 %copy-start.9 = (u32[32]{0:T(128)S(1)}, u32[32]{0:T(128)}, u32[]{:S(2)}) copy-start(u32[32]{0:T(128)} %constant.96) | copy-start | bytes 388
  137.5 11.3 %all-to-all-start.5 = ((bf16[4,7,4096]{2,1,0:T(8,128)(2,1)}), bf16[4,7,4096]{2,1,0:T(8,128)(2,1)S(1)}, u32[]{:S(2)}, u32[]{:S(2)}) async-start(bf16[4,7,4096]{2,1,0:T(8,128)(2,1)} %all_to_all.67), calls=%async_computation.5 | async-start | bytes 524288 | tf_op jit(solution)/shard_map/all_to_all | solution.py:176
  140.9 59.6 %all-reduce.6.cloned.1.call-start = ((), (), s32[]{:S(2)}) async-start(), calls=%async_computation.7 | async-start | bytes 131072
Sparse Core Ops, SparseCore 0:
  64.2 52.5 all-reduce.3
  150.0 50.4 all-reduce.5
where the time goes:
time: 213 us; the launch traced here: 212 us
  waiting for transfers between devices  122 us (57%)
  matrix products  21.2 us (10%)
  starting transfers between devices  19.6 us (9%)
  between operations  16.4 us (8%)
  other arithmetic  12.9 us (6%)
  blocking collectives  12.5 us (6%)
  local copies, waits for them, and re-layouts  7.42 us (3%)
    psum x1, waiting for transfers between devices, on_device(): mixed = lax.psum(head_term.astype(jnp.bfloat16), 'tp').astype(jnp.float32)  52.6 us
    unnamed x3, waiting for transfers between devices  48.9 us
    all_to_all x1, blocking collectives, on_device(): lax.all_to_all(outgoing, 'ep', split_axis=0, concat_axis=0, tiled=True)  12.5 us
    all_to_all x1, waiting for transfers between devices, on_device(): lax.all_to_all(expert_out, 'ep', split_axis=0, concat_axis=0, tiled=True)  7.75 us
    reduce_sum x5, other arithmetic, rms_scale(): jnp.mean(values_f * values_f, axis=-1, keepdims=True) + EPSILON  5.68 us
    all_to_all x1, starting transfers between devices, on_device(): lax.all_to_all(latent_cols, 'tp', split_axis=0, concat_axis=1, tiled=True)  5.2 us
    all_to_all x1, waiting for transfers between devices, on_device(): lax.all_to_all(attended.reshape(seq_count, -1), 'tp', split_axis=1, conca...  4.81 us
    all_to_all x1, waiting for transfers between devices, on_device(): lax.all_to_all(q_latent, 'tp', split_axis=0, concat_axis=1, tiled=True)  4.75 us
  transfers between devices with their start and end apart: 7, of which 6 were waited for; matrix products, arithmetic and copies ran while one was open for 6% of the time, Pallas kernels for 0%

commit v1 on v0

--- a/solution.py
+++ b/solution.py
@@ -6,6 +6,11 @@
 EXP_LOCAL = 1
 EPSILON = 1e-06
 ROTARY_BASE = 500000.0
+
+
+def add_all(x, axis):
+    pieces = lax.all_gather(x, axis)
+    return jnp.sum(pieces, axis=0)
 
 
 def rms_scale(source, gain_row):
@@ -137,7 +142,7 @@
         .reshape(group_rows, -1)
     )
     head_term = jnp.dot(values, w_output, preferred_element_type=jnp.float32)
-    mixed = lax.psum(head_term.astype(jnp.bfloat16), "tp").astype(jnp.float32)
+    mixed = add_all(head_term.astype(jnp.bfloat16), "tp").astype(jnp.float32)
     resid = (tokens.astype(jnp.float32) + rms_scale(mixed, norm_gains[1])).astype(jnp.bfloat16)
     expert_in = rms_scale(resid, norm_gains[2]).astype(jnp.bfloat16)
     own_resid = lax.dynamic_slice_in_dim(resid, tp_rank * seq_count, seq_count, 0)

time: 213 us -> 170 us (0.80)
  waiting for transfers between devices: 122 us -> 70.3 us
  blocking collectives: 12.5 us -> 22.9 us
    psum x1 -> x0, waiting for transfers between devices: 52.6 us -> none  [on_device(): mixed = lax.psum(head_term.astype(jnp.bfloat16), 'tp').astype(jnp.float32)]
    all_gather x0 -> x1, blocking collectives: none -> 8.88 us  [add_all(): pieces = lax.all_gather(x, axis)]
    unnamed x3 -> x2, waiting for transfers between devices: 48.9 us -> 49.5 us
  transfers between devices with their start and end apart: 7 -> 6, of which waited for: 6 -> 5; matrix products, arithmetic and copies ran while one was open for 6% -> 8% of each run, Pallas kernels for 0% -> 0%
where the time goes in v1:
time: 170 us; the launch traced here: 169 us
  waiting for transfers between devices  70.3 us (41%)
  blocking collectives  22.9 us (13%)
  matrix products  20.6 us (12%)
  starting transfers between devices  19.5 us (11%)
  between operations  16.4 us (10%)
  other arithmetic  11.4 us (7%)
  local copies, waits for them, and re-layouts  7.42 us (4%)
    unnamed x2, waiting for transfers between devices  49.5 us
    all_to_all x1, blocking collectives, on_device(): lax.all_to_all(outgoing, 'ep', split_axis=0, concat_axis=0, tiled=True)  14.1 us
    all_gather x1, blocking collectives, add_all(): pieces = lax.all_gather(x, axis)  8.88 us
    all_to_all x1, waiting for transfers between devices, on_device(): lax.all_to_all(expert_out, 'ep', split_axis=0, concat_axis=0, tiled=True)  7.88 us
    all_to_all x1, starting transfers between devices, on_device(): lax.all_to_all(latent_cols, 'tp', split_axis=0, concat_axis=1, tiled=True)  5.2 us
    all_to_all x1, waiting for transfers between devices, on_device(): lax.all_to_all(attended.reshape(seq_count, -1), 'tp', split_axis=1, conca...  4.87 us
    all_to_all x1, waiting for transfers between devices, on_device(): lax.all_to_all(q_latent, 'tp', split_axis=0, concat_axis=1, tiled=True)  4.75 us
    all_to_all x1, starting transfers between devices, on_device(): lax.all_to_all(q_rot, 'tp', split_axis=0, concat_axis=1, tiled=True)  4.2 us
  transfers between devices with their start and end apart: 6, of which 5 were waited for; matrix products, arithmetic and copies ran while one was open for 8% of the time, Pallas kernels for 0%

profile of v1, /device:TPU:0, one launch (start us, length us, event | category | flops | bytes accessed | tf_op | source)
XLA Modules:
  0.0 168.6 jit_solution(14218468985177757310)
XLA Ops:
  7.2 1.1 fusion.78
  8.3 1.1 fusion.40
  9.4 0.9 fusion.42
  10.3 1.5 fusion.29
  11.8 0.6 copy.35
  12.4 5.2 %all-to-all-start.2 = ((bf16[8,1,128]{2,1,0:T(2,128)(2,1)}), bf16[8,1,128]{2,1,0:T(2,128)(2,1)S(1)}, u32[]{:S(2)}, u32[]{:S(2)}) async-start(bf16[8,1,128]{2,1,0:T(2,128)(2,1)} %copy.35), calls=%async_computation.2 | async-start | bytes 8192 | tf_op jit(solution)/shard_map/all_to_all | solution.py:106
  17.6 2.0 %fusion.28 = bf16[8,1,256]{2,0,1:T(8,128)(2,1)S(1)} fusion(bf16[8,4096]{1,0:T(8,128)(2,1)S(1)} %fusion.42, bf16[4096,256]{1,0:T(8,128)(2,1)} %param.21), kind=kOutput, calls=%fused_computation.28 | convolution fusion | flops 16779264 | bytes 2166784 | tf_op jit(solution)/shard_map/dot_general | solution.py:99
  20.3 1.3 fusion.34
  22.0 0.2 select_reduce_fusion.1
  22.2 3.1 %convolution_convert_fusion.3 = bf16[4,8,1024]{2,1,0:T(8,128)(2,1)S(1)} fusion(bf16[4,128,1024]{2,1,0:T(8,128)(2,1)S(1)} %copy-done.2, bf16[8,4096]{1,0:T(8,128)(2,1)S(1)} %fusion.42, bf16[4096,512]{1,0:T(8,128)(2,1)} %param.20), kind=kOutput, calls=%fused_computation.20 | convolution fusion | flops 41979904 | bytes 5373952 | tf_op jit(solution)/shard_map/thn,hnc->thc/dot_general | solution.py:97
  25.3 0.5 broadcast.263
  25.8 0.6 reduce.14
  26.5 0.6 reshape.356
  27.1 0.7 reduce.13
  27.8 0.7 reshape.354
  28.5 4.2 %all-to-all-start.1 = ((bf16[8,2,128]{2,1,0:T(2,128)(2,1)}), bf16[8,2,128]{2,1,0:T(2,128)(2,1)S(1)}, u32[]{:S(2)}, u32[]{:S(2)}) async-start(bf16[8,2,128]{2,1,0:T(2,128)(2,1)} %reshape.356), calls=%async_computation.1 | async-start | bytes 8192 | tf_op jit(solution)/shard_map/all_to_all | solution.py:105
  32.7 0.6 multiply_reduce_fusion.1
  34.1 3.3 %all-to-all-done.1 = bf16[8,2,128]{2,1,0:T(2,128)(2,1)S(1)} async-done(((bf16[8,2,128]{2,1,0:T(2,128)(2,1)}), bf16[8,2,128]{2,1,0:T(2,128)(2,1)S(1)}, u32[]{:S(2)}, u32[]{:S(2)}) %all-to-all-start.1) | async-done | bytes 4128 | tf_op jit(solution)/shard_map/all_to_all | solution.py:105
  37.3 3.3 %all-to-all-start = ((bf16[8,2,2048]{2,1,0:T(2,128)(2,1)}), bf16[8,2,2048]{2,1,0:T(2,128)(2,1)S(1)}, u32[]{:S(2)}, u32[]{:S(2)}) async-start(bf16[8,2,2048]{2,1,0:T(2,128)(2,1)} %reshape.354), calls=%async_computation | async-start | bytes 131072 | tf_op jit(solution)/shard_map/all_to_all | solution.py:104
  40.9 4.8 %all-to-all-done = bf16[8,2,2048]{2,1,0:T(2,128)(2,1)S(1)} async-done(((bf16[8,2,2048]{2,1,0:T(2,128)(2,1)}), bf16[8,2,2048]{2,1,0:T(2,128)(2,1)S(1)}, u32[]{:S(2)}, u32[]{:S(2)}) %all-to-all-start) | async-done | bytes 65568 | tf_op jit(solution)/shard_map/all_to_all | solution.py:104
  45.7 0.4 reduce.8
  46.1 2.5 %fusion.9 = f32[32,1024]{1,0:T(8,128)S(1)} fusion(bf16[32,1024]{1,0:T(8,128)(2,1)S(1)} %reshape.334, bf16[1,1024,1024]{2,1,0:T(8,128)(2,1)} %param.28), kind=kOutput, calls=%fused_computation.14 | convolution fusion | flops 67108864 | bytes 2293760 | tf_op jit(solution)/shard_map/shc,spc->shp/dot_general | solution.py:42
  48.7 0.3 select_reduce_fusion
  49.1 0.2 fusion.79
  49.3 0.2 fusion.45
  49.5 0.5 fusion.15
  50.1 1.0 reduce.15
  51.1 0.7 reshape.358
  51.8 3.3 %all-to-all-start.3 = ((bf16[8,2,2048]{2,1,0:T(2,128)(2,1)}), bf16[8,2,2048]{2,1,0:T(2,128)(2,1)S(1)}, u32[]{:S(2)}, u32[]{:S(2)}) async-start(bf16[8,2,2048]{2,1,0:T(2,128)(2,1)} %reshape.358), calls=%async_computation.3 | async-start | bytes 131072 | tf_op jit(solution)/shard_map/all_to_all | solution.py:131
  55.2 4.9 %all-to-all-done.3 = bf16[8,2,2048]{2,1,0:T(2,128)(2,1)S(1)} async-done(((bf16[8,2,2048]{2,1,0:T(2,128)(2,1)}), bf16[8,2,2048]{2,1,0:T(2,128)(2,1)S(1)}, u32[]{:S(2)}, u32[]{:S(2)}) %all-to-all-start.3) | async-done | bytes 65568 | tf_op jit(solution)/shard_map/all_to_all | solution.py:131
  60.1 0.4 bitcast_reduce_fusion.1
  60.5 3.1 %convolution_convert_fusion.2 = bf16[8,4096]{1,0:T(8,128)(2,1)S(1)} fusion(bf16[512,4096]{1,0:T(8,128)(2,1)} %param.24, bf16[8,4,1024]{2,0,1:T(8,128)(2,1)S(1)} %bitcast.125, bf16[4,1024,128]{2,1,0:T(8,128)(2,1)S(1)} %copy-done.3), kind=kOutput, calls=%fused_computation.6 | convolution fusion | flops 41979904 | bytes 5373952 | tf_op jit(solution)/shard_map/dot_general | solution.py:144
  63.6 8.9 %all-gather = bf16[64,4096]{1,0:T(8,128)(2,1)S(1)} all-gather(bf16[8,4096]{1,0:T(8,128)(2,1)S(1)} %convolution_convert_fusion.2), channel_id=2, replica_groups=mesh['ep'=4,'tp'=8] {'tp'}, dimensions={0}, use_global_device_ids=true | all-gather | bytes 589824 | tf_op jit(solution)/shard_map/all_gather | solution.py:12
  72.7 0.2 fusion.37
  72.9 0.3 convolution_convert_fusion.1
  73.3 14.1 %all_to_all.77 = bf16[4,7,4096]{2,1,0:T(8,128)(2,1)S(1)} all-to-all(bf16[4,7,4096]{2,1,0:T(8,128)(2,1)S(1)} %all_to_all.64), channel_id=1, replica_groups=mesh['ep'=4,'tp'=8] {'ep'}, dimensions={0} | all-to-all | bytes 458752 | tf_op jit(solution)/shard_map/all_to_all | solution.py:174
  87.5 2.1 %fusion.5 = f32[28,256]{1,0:T(8,128)S(1)} fusion(bf16[28,4096]{1,0:T(8,128)(2,1)S(1)} %all_to_all.66, bf16[1,4096,256]{2,1,0:T(8,128)(2,1)} %param.33), kind=kOutput, calls=%fused_computation.10 | convolution fusion | flops 58720256 | bytes 2355200 | tf_op jit(solution)/shard_map/dot_general | solution.py:175
  89.5 2.9 %convolution_convert_fusion = bf16[28,4096]{1,0:T(8,128)(2,1)S(1)} fusion(bf16[1,256,4096]{2,1,0:T(8,128)(2,1)S(1)} %copy-done, bf16[28,4096]{1,0:T(8,128)(2,1)S(1)} %all_to_all.66, bf16[1,4096,256]{2,1,0:T(8,128)(2,1)} %param.34, f32[28,256]{1,0:T(8,128)S(1)} %fusion.5), kind=kOutput, calls=%fused_computation | convolution fusion | flops 117598208 | bytes 4681728 | tf_op jit(solution)/shard_map/dot_general | solution.py:178
  92.4 0.8 all_to_all.67
  93.2 3.4 %all-to-all-start.5 = ((bf16[4,7,4096]{2,1,0:T(8,128)(2,1)}), bf16[4,7,4096]{2,1,0:T(8,128)(2,1)S(1)}, u32[]{:S(2)}, u32[]{:S(2)}) async-start(bf16[4,7,4096]{2,1,0:T(8,128)(2,1)} %all_to_all.67), calls=%async_computation.5 | async-start | bytes 524288 | tf_op jit(solution)/shard_map/all_to_all | solution.py:181
  96.7 7.9 %all-to-all-done.5 = bf16[4,7,4096]{2,1,0:T(8,128)(2,1)S(1)} async-done(((bf16[4,7,4096]{2,1,0:T(8,128)(2,1)}), bf16[4,7,4096]{2,1,0:T(8,128)(2,1)S(1)}, u32[]{:S(2)}, u32[]{:S(2)}) %all-to-all-start.5) | async-done | bytes 229408 | tf_op jit(solution)/shard_map/all_to_all | solution.py:181
  104.9 0.8 fusion.1
  105.7 0.6 pad_maximum_fusion.3
  106.3 0.6 dynamic-slice
  106.8 0.6 convert_element_type.186
  107.4 49.5 %all-reduce.3.cloned.1.call-done = bf16[8,4096]{1,0:T(8,128)(2,1)} async-done(((bf16[8,4096]{1,0:T(8,128)(2,1)}), bf16[8,4096]{1,0:T(8,128)(2,1)}) %all-reduce.3.cloned.1.call-update) | async-done | bytes 65552
  157.0 2.0 %multiply_reduce_fusion = f32[]{:T(128)} fusion(bf16[8,4096]{1,0:T(8,128)(2,1)} %all-reduce.3.cloned.1.call-done, u32[]{:T(128)} %bitcast.36), kind=kLoop, calls=%fused_computation.75 | loop fusion | flops 12287 | bytes 8200 | tf_op jit(solution)/shard_map/reduce_sum | solution.py:20
  159.7 2.1 %add_convert_fusion = bf16[1,4096]{1,0:T(2,128)(2,1)} fusion(f32[4,4096]{1,0:T(4,128)} %param.19, bf16[8,4096]{1,0:T(8,128)(2,1)S(1)} %get-tuple-element.4, s32[]{:T(128)S(6)} %select_n.40, bf16[8,4096]{1,0:T(8,128)(2,1)} %all-reduce.3.cloned.1.call-done, u32[]{:T(128)} %bitcast.36, f32[]{:T(128)S(6)} %rsqrt.36), kind=kLoop, calls=%fused_computation.74 | loop fusion | flops 24576 | bytes 40972 | tf_op jit(solution)/shard_map/convert_element_type | solution.py:189
  (58 shorter events, 2.1 us)
Async XLA Ops:
  7.2 82.3 %copy-start = (bf16[1,256,4096]{2,1,0:T(8,128)(2,1)S(1)}, bf16[1,256,4096]{2,1,0:T(8,128)(2,1)}, u32[]{:S(2)}) copy-start(bf16[1,256,4096]{2,1,0:T(8,128)(2,1)} %param.35) | copy-start | bytes 6291460
  7.2 14.5 %copy-start.7 = (s32[8,2]{0,1:T(2,128)S(1)}, s32[8,2]{0,1:T(2,128)}, u32[]{:S(2)}) copy-start(s32[8,2]{0,1:T(2,128)} %param.31) | copy-start | bytes 196
  8.3 13.9 %copy-start.2 = (bf16[4,128,1024]{2,1,0:T(8,128)(2,1)S(1)}, bf16[4,128,1024]{2,1,0:T(8,128)(2,1)}, u32[]{:S(2)}) copy-start(bf16[4,128,1024]{2,1,0:T(8,128)(2,1)} %param.22) | copy-start | bytes 3145732
  12.4 16.1 %all-to-all-start.2 = ((bf16[8,1,128]{2,1,0:T(2,128)(2,1)}), bf16[8,1,128]{2,1,0:T(2,128)(2,1)S(1)}, u32[]{:S(2)}, u32[]{:S(2)}) async-start(bf16[8,1,128]{2,1,0:T(2,128)(2,1)} %copy.35), calls=%async_computation.2 | async-start | bytes 8192 | tf_op jit(solution)/shard_map/all_to_all | solution.py:106
  22.2 11.8 %copy-start.6 = (f32[1024]{0:T(1024)S(1)}, f32[1024]{0:T(1024)}, u32[]{:S(2)}) copy-start(f32[1024]{0:T(1024)} %param.26) | copy-start | bytes 12292
  25.3 23.4 %copy-start.5 = (bf16[1,1024,64]{1,2,0:T(8,128)(2,1)S(1)}, bf16[1,1024,64]{1,2,0:T(8,128)(2,1)}, u32[]{:S(2)}) copy-start(bf16[1,1024,64]{1,2,0:T(8,128)(2,1)} %param.29) | copy-start | bytes 393220
  28.5 8.8 %all-to-all-start.1 = ((bf16[8,2,128]{2,1,0:T(2,128)(2,1)}), bf16[8,2,128]{2,1,0:T(2,128)(2,1)S(1)}, u32[]{:S(2)}, u32[]{:S(2)}) async-start(bf16[8,2,128]{2,1,0:T(2,128)(2,1)} %reshape.356), calls=%async_computation.1 | async-start | bytes 8192 | tf_op jit(solution)/shard_map/all_to_all | solution.py:105
  37.3 8.3 %all-to-all-start = ((bf16[8,2,2048]{2,1,0:T(2,128)(2,1)}), bf16[8,2,2048]{2,1,0:T(2,128)(2,1)S(1)}, u32[]{:S(2)}, u32[]{:S(2)}) async-start(bf16[8,2,2048]{2,1,0:T(2,128)(2,1)} %reshape.354), calls=%async_computation | async-start | bytes 131072 | tf_op jit(solution)/shard_map/all_to_all | solution.py:104
  46.1 3.4 %copy-start.1 = (bf16[1,1024,1024]{2,1,0:T(8,128)(2,1)S(1)}, bf16[1,1024,1024]{2,1,0:T(8,128)(2,1)}, u32[]{:S(2)}) copy-start(bf16[1,1024,1024]{2,1,0:T(8,128)(2,1)} %param.28) | copy-start | bytes 6291460
  48.6 11.9 %copy-start.3 = (bf16[4,1024,128]{2,1,0:T(8,128)(2,1)S(1)}, bf16[4,1024,128]{2,1,0:T(8,128)(2,1)}, u32[]{:S(2)}) copy-start(bf16[4,1024,128]{2,1,0:T(8,128)(2,1)} %param.23) | copy-start | bytes 3145732
  51.8 8.3 %all-to-all-start.3 = ((bf16[8,2,2048]{2,1,0:T(2,128)(2,1)}), bf16[8,2,2048]{2,1,0:T(2,128)(2,1)S(1)}, u32[]{:S(2)}, u32[]{:S(2)}) async-start(bf16[8,2,2048]{2,1,0:T(2,128)(2,1)} %reshape.358), calls=%async_computation.3 | async-start | bytes 131072 | tf_op jit(solution)/shard_map/all_to_all | solution.py:131
  60.5 12.2 %copy-start.4 = (bf16[8,4096]{1,0:T(8,128)(2,1)S(1)}, bf16[8,4096]{1,0:T(8,128)(2,1)}, u32[]{:S(2)}) copy-start(bf16[8,4096]{1,0:T(8,128)(2,1)} %param.18) | copy-start | bytes 196612
  89.5 7.1 %copy-start.8 = (f32[8,2]{0,1:T(2,128)S(1)}, f32[8,2]{0,1:T(2,128)}, u32[]{:S(2)}) copy-start(f32[8,2]{0,1:T(2,128)} %param.32) | copy-start | bytes 196
  92.4 13.9 %copy-start.9 = (u32[32]{0:T(128)S(1)}, u32[32]{0:T(128)}, u32[]{:S(2)}) copy-start(u32[32]{0:T(128)} %constant.97) | copy-start | bytes 388
  93.2 11.4 %all-to-all-start.5 = ((bf16[4,7,4096]{2,1,0:T(8,128)(2,1)}), bf16[4,7,4096]{2,1,0:T(8,128)(2,1)S(1)}, u32[]{:S(2)}, u32[]{:S(2)}) async-start(bf16[4,7,4096]{2,1,0:T(8,128)(2,1)} %all_to_all.67), calls=%async_computation.5 | async-start | bytes 524288 | tf_op jit(solution)/shard_map/all_to_all | solution.py:181
  96.6 60.4 %all-reduce.3.cloned.1.call-start = ((), (), s32[]{:S(2)}) async-start(), calls=%async_computation.6 | async-start | bytes 131072
Sparse Core Ops, SparseCore 0:
  105.8 51.1 all-reduce.2
